TPU v7x, 32 devices: a whole 2x2x4 slice. The times are simulated.
32 devices in a mesh: sp: 8 (over z, x), tp: 4 (over y, core).
Axes of the slice: x: 2, y: 2, z: 4, core: 2. Of those that a mesh axis runs over, the one named last changes fastest.
Arguments:
- residual_matrix: bfloat16 [2048, 2048], P(('sp', 'tp')), may hold values from -6 to 6
- query_vectors: bfloat16 [2048, 2048], P('tp', 'sp'), may hold values from -6 to 6
- lookup_vectors: bfloat16 [2048, 2048], P('tp', 'sp'), may hold values from -6 to 6
- payload_vectors: bfloat16 [2048, 2048], P('tp', 'sp'), may hold values from -6 to 6
- fading_dependent_term: bfloat16 [2048, 2048], P('tp', 'sp'), may hold values from -4 to 4
- step_size_preactivation: bfloat16 [2048, 2048], P('tp', 'sp'), may hold values from -8 to 8
- attention_result_switch: bfloat16 [2048, 2048], P('tp', 'sp'), may hold values from -6 to 6
- fading_bias_vector: float32 [2048], P('tp'), may hold values from -16 to -2
- surplus_forgetting: float32 [32, 2048], P('tp', 'sp'), may hold values from -0.7 to 0
- per_group_scaler: float32 [2048], P('tp'), may hold values from 0.1 to 1.9
- attention_result_matrix: bfloat16 [2048, 2048], P('tp'), may hold values from -0.125 to 0.125
- dense_block_scaler: float32 [2048], replicated, may hold values from 0.1 to 1.9
- switching_matrix: bfloat16 [2048, 5632], P('sp', 'tp'), may hold values from -0.125 to 0.125
- expanding_matrix: bfloat16 [2048, 5632], P('sp', 'tp'), may hold values from -0.125 to 0.125
- contracting_matrix: bfloat16 [5632, 2048], P('tp', 'sp'), may hold values from -0.078125 to 0.078125
Outputs:
- blended: bfloat16 [2048, 2048], P(('sp', 'tp'))
All inputs are finite; a program needn't handle non-finite values.
Results may differ from a plain program's by a relative error of at most 0.015.
Values may be sent and summed in bfloat16 or wider, within the bound.
A program may use at most 128 MiB of HBM per device.

v0:
```python
import functools
import jax
import jax.numpy as jnp
from jax import lax
from jax.experimental import pallas as pl
from jax.experimental.pallas import tpu as pltpu
from jax.sharding import PartitionSpec as P

HEAD = 64
BLOCK = 64


norm_eps = 1e-06
group_eps = 0.00064
key_eps = 1e-06
highest = lax.Precision.HIGHEST
high = lax.Precision.HIGH


def shifted(x, axis, by):
    n = lax.axis_size(axis)
    return lax.ppermute(x, axis, [(i, (i + by) % n) for i in range(n)])


def paired(x):
    n = lax.axis_size("sp")
    return lax.ppermute(x, "sp", [(i, i ^ 1) for i in range(n)])


def around(first, second):
    n = lax.axis_size("sp")
    ring = n // 2
    half = ring // 2

    def hop(x, by):
        return lax.ppermute(x, "sp", [(i, (i + 2 * by) % n) for i in range(n)])

    out = [[None] * ring, [None] * ring]
    for place, piece in enumerate((first, second)):
        out[place][0] = piece
        up = down = piece
        for step in range(1, half):
            up = hop(up, 1)
            down = hop(down, -1)
            out[place][ring - step] = up
            out[place][step] = down
        if ring > 1:
            out[place][half] = hop(up, 1) if place == 0 else hop(down, -1)
    return out


def rolled(x, by):
    return lax.dynamic_slice_in_dim(jnp.concatenate([x, x], axis=1), by, x.shape[1], 1)


def carried_in(summary):
    n = lax.axis_size("sp")
    carry_map, carry_add = summary
    both = jnp.concatenate([carry_map, carry_add], axis=1).astype(jnp.bfloat16)
    width = carry_map.shape[1]
    state = jnp.zeros_like(carry_add)
    for back in range(n - 1, 0, -1):
        came = lax.ppermute(both, "sp", [(i, i + back) for i in range(n - back)])
        came = came.astype(jnp.float32)
        state = (
            jnp.einsum("hvk,hkj->hvj", state, came[:, :width], precision=high)
            + came[:, width:]
        )
    return state


def by_blocks(source, attention_group_count, position_count):
    return (
        source.astype(jnp.float32)
        .reshape(attention_group_count, HEAD, position_count // BLOCK, BLOCK)
        .transpose(0, 2, 3, 1)
    )


def compose(earlier, latter):
    return (
        jnp.einsum("...ij,...jk->...ik", earlier[0], latter[0], precision=high),
        jnp.einsum("...ij,...jk->...ik", earlier[1], latter[0], precision=high) + latter[1],
    )


def unit_lower_solve(mutual, right_side):
    power = -mutual
    solved = right_side
    for level in range((BLOCK - 1).bit_length()):
        solved = solved + jnp.einsum("hbts,hbsn->hbtn", power, solved, precision=highest)
        if level + 1 < (BLOCK - 1).bit_length():
            power = jnp.einsum("hbts,hbsu->hbtu", power, power, precision=highest)
    return solved


def rms_rows(middle, dense_block_scaler):
    scale_rows = lax.rsqrt(jnp.mean(middle * middle, axis=-1, keepdims=True) + norm_eps)
    return (middle * scale_rows * dense_block_scaler).astype(jnp.bfloat16)


def local(
    residual_matrix,
    query_vectors,
    lookup_vectors,
    payload_vectors,
    fading_dependent_term,
    step_size_preactivation,
    attention_result_switch,
    fading_bias_vector,
    surplus_forgetting,
    per_group_scaler,
    attention_result_matrix,
    dense_block_scaler,
    switching_matrix,
    expanding_matrix,
    contracting_matrix,
):
    count_sp, count_tp = lax.axis_size("sp"), lax.axis_size("tp")
    parity = lax.axis_index("sp") % 2
    ring_place = lax.axis_index("sp") // 2
    units = switching_matrix.shape[1] // 2

    def part(x, which, axis):
        return lax.dynamic_slice_in_dim(x, which * units, units, axis)

    def gate_up(which):
        return jnp.concatenate(
            [part(switching_matrix, which, 1), part(expanding_matrix, which, 1)], axis=1
        )

    wide_pieces = around(gate_up(parity), paired(gate_up(1 - parity)))
    down_pieces = around(
        part(contracting_matrix, parity, 0), part(contracting_matrix, 1 - parity, 0)
    )
    attention_group_count = surplus_forgetting.shape[0]
    position_count = surplus_forgetting.shape[1]
    block_count = position_count // BLOCK
    read_rows = by_blocks(query_vectors, attention_group_count, position_count)
    key_rows = by_blocks(lookup_vectors, attention_group_count, position_count)
    value_rows = by_blocks(payload_vectors, attention_group_count, position_count)
    fading_preactivation = by_blocks(
        fading_dependent_term, attention_group_count, position_count
    ) + fading_bias_vector.reshape(attention_group_count, 1, 1, HEAD)
    log_fading_factor = -jnp.exp(
        -jax.nn.softplus(-fading_preactivation) - 0.5
    ) + surplus_forgetting.reshape(attention_group_count, block_count, BLOCK, 1)
    learn_rate = jax.nn.sigmoid(
        by_blocks(step_size_preactivation, attention_group_count, position_count)
    )
    unit_keys = key_rows * lax.rsqrt(jnp.sum(key_rows * key_rows, axis=-1, keepdims=True) + key_eps)
    scaled = key_rows * learn_rate
    removal = unit_keys * learn_rate
    cum_after = jnp.cumsum(log_fading_factor, axis=2)
    before = cum_after - log_fading_factor
    cum_final = cum_after[:, :, -1:, :]
    probe_keys = unit_keys * jnp.exp(before)
    removal_in = removal * jnp.exp(-cum_after)
    scaled_in = scaled * jnp.exp(-cum_after)
    reads_out = read_rows * jnp.exp(cum_after)
    position = jnp.arange(BLOCK)
    strict = position[:, None] > position[None, :]
    up_to = position[:, None] >= position[None, :]
    mutual = jnp.where(
        strict, jnp.einsum("hbtn,hbsn->hbts", probe_keys, removal_in, precision=high), 0.0
    )
    through = jnp.where(
        strict, jnp.einsum("hbtn,hbsn->hbts", probe_keys, scaled_in, precision=high), 0.0
    )
    right_side = jnp.concatenate(
        [probe_keys, jnp.einsum("hbts,hbsn->hbtn", through, value_rows, precision=high)], axis=-1
    )
    solved = unit_lower_solve(mutual, right_side)
    basis_part = solved[..., :HEAD]
    offset = solved[..., HEAD:]
    removal_end = removal * jnp.exp(cum_final - cum_after)
    scaled_end = scaled * jnp.exp(cum_final - cum_after)
    carry_map = jnp.eye(HEAD, dtype=jnp.float32) * jnp.exp(cum_final) - jnp.einsum(
        "hbtk,hbtj->hbkj", basis_part, removal_end, precision=high
    )
    carry_add = jnp.einsum(
        "hbtv,hbtj->hbvj", value_rows, scaled_end, precision=high
    ) - jnp.einsum("hbtv,hbtj->hbvj", offset, removal_end, precision=high)
    summary = (carry_map[:, 0], carry_add[:, 0])
    for block in range(1, block_count):
        summary = compose(summary, (carry_map[:, block], carry_add[:, block]))
    carried = carried_in(summary)
    starts = [carried]
    for block in range(block_count - 1):
        carried = (
            jnp.einsum("hvk,hkj->hvj", carried, carry_map[:, block], precision=high)
            + carry_add[:, block]
        )
        starts.append(carried)
    starts = jnp.stack(starts, axis=1)
    removed = -jnp.einsum("hbtk,hbvk->hbtv", basis_part, starts, precision=high) - offset
    reach_removal = jnp.where(
        up_to, jnp.einsum("hbtn,hbsn->hbts", reads_out, removal_in, precision=high), 0.0
    )
    reach_value = jnp.where(
        up_to, jnp.einsum("hbtn,hbsn->hbts", reads_out, scaled_in, precision=high), 0.0
    )
    outputs = (
        jnp.einsum("hbtk,hbvk->hbtv", reads_out, starts, precision=high)
        + jnp.einsum("hbts,hbsv->hbtv", reach_removal, removed, precision=high)
        + jnp.einsum("hbts,hbsv->hbtv", reach_value, value_rows, precision=high)
    )
    centred = outputs - jnp.mean(outputs, axis=-1, keepdims=True)
    normed_heads = centred * lax.rsqrt(
        jnp.mean(centred * centred, axis=-1, keepdims=True) + group_eps
    )
    normed_heads = normed_heads.transpose(0, 3, 1, 2).reshape(
        attention_group_count * HEAD, position_count
    )
    mixed_out = (
        normed_heads * per_group_scaler[:, None] * attention_result_switch.astype(jnp.float32)
    ).astype(jnp.bfloat16)
    tp_place = lax.axis_index("tp")
    rows = residual_matrix.shape[0]
    partial = jnp.einsum(
        "ct,cd->td", mixed_out, attention_result_matrix, preferred_element_type=jnp.float32
    )

    def rows_of(x, by):
        owner = (tp_place + by) % count_tp
        return lax.dynamic_slice_in_dim(x, owner * rows, rows, 0)

    sent = partial.astype(jnp.bfloat16)
    middle = residual_matrix.astype(jnp.float32) + rows_of(partial, 0)
    for by in range(1, count_tp):
        middle = middle + shifted(rows_of(sent, by), "tp", by).astype(jnp.float32)
    normed = rms_rows(middle, dense_block_scaler)
    depth = switching_matrix.shape[0]

    def column_blocks(x):
        return [x[:, i * depth : (i + 1) * depth] for i in range(x.shape[1] // depth)]

    turned = rolled(normed, ring_place * 2 * depth)
    blocks = column_blocks(turned)
    flipped = jnp.concatenate([blocks[i ^ 1] for i in range(count_sp)], axis=1)
    near = jnp.where(parity == 0, turned, flipped)
    far = paired(jnp.where(parity == 0, flipped, turned))

    def spread(x):
        return jnp.concatenate([x] + [shifted(x, "tp", by) for by in range(1, count_tp)], axis=0)

    def stacked(pieces):
        return jnp.concatenate([x for pair in zip(*pieces) for x in pair], axis=0)

    wide_weight = stacked(wide_pieces)

    def units_of(x):
        both = jnp.dot(x, wide_weight, preferred_element_type=jnp.float32)
        return (jax.nn.silu(both[:, :units]) * both[:, units:]).astype(jnp.bfloat16)

    near_units = units_of(spread(near))
    near_sent = paired(near_units)
    far_units = units_of(spread(far))
    far_sent = paired(far_units)
    down_own = jnp.concatenate(down_pieces[0], axis=1)
    down_other = jnp.concatenate(down_pieces[1], axis=1)

    def summed(own, other):
        product = (
            jnp.dot(own, down_own, preferred_element_type=jnp.float32)
            + jnp.dot(other, down_other, preferred_element_type=jnp.float32)
        ).astype(jnp.bfloat16)
        total = product[:rows].astype(jnp.float32)
        for by in range(1, count_tp):
            total = total + shifted(product[by * rows : (by + 1) * rows], "tp", -by).astype(
                jnp.float32
            )
        return total

    far_sum = paired(summed(far_units, near_sent).astype(jnp.bfloat16)).astype(jnp.float32)
    near_sum = summed(near_units, far_sent)
    even = column_blocks(jnp.where(parity == 0, near_sum, far_sum))
    odd = column_blocks(jnp.where(parity == 0, far_sum, near_sum))
    columns = jnp.concatenate([x for pair in zip(even, odd) for x in pair], axis=1)
    channel_out = rolled(columns, (count_sp // 2 - ring_place) % (count_sp // 2) * 2 * depth)
    return (middle + channel_out).astype(jnp.bfloat16)


LANES = 128
PAIR = 2
MESH = pl.DeviceIdType.MESH
f32, bf16 = jnp.float32, jnp.bfloat16
NN = (((1,), (0,)), ((), ()))
NT = (((1,), (1,)), ((), ()))


def mm(a, b, dims=NN):
    return lax.dot_general(a, b, dims, preferred_element_type=f32)


def split(x):
    top = x.astype(bf16)
    return top, (x - top.astype(f32)).astype(bf16)


def mm3(a, b, dims=NN):
    (ah, al), (bh, bl) = split(a), split(b)
    return mm(ah, bh, dims) + mm(ah, bl, dims) + mm(al, bh, dims)


def mm2(a, b, dims=NN):
    bh, bl = split(b)
    return mm(a, bh, dims) + mm(a, bl, dims)


def grid_of(rows):
    return (
        lax.broadcasted_iota(jnp.int32, (rows, LANES), 0),
        lax.broadcasted_iota(jnp.int32, (rows, LANES), 1),
    )


def heads_apart(x):
    row, col = grid_of(LANES)
    return jnp.where((row < HEAD) == (col < HEAD), jnp.concatenate([x, x], axis=0), 0.0)


def inverses(mutuals):
    row, col = grid_of(LANES)
    eye = jnp.where(row == col, 1.0, 0.0)
    solved = [eye - jnp.where((row % 2 == 0) & (col == row + 1), a, 0.0) for a in mutuals]
    for level in range(1, LANES.bit_length() - 1):
        size = 1 << level
        cross = ((row // size) % 2 == 0) & (col // size == row // size + 1)
        rounded = [s.astype(bf16) for s in solved]
        moved = [
            mm(r, jnp.where(cross, a, 0.0).astype(bf16)).astype(bf16)
            for r, a in zip(rounded, mutuals)
        ]
        solved = [s - mm(m, r) for s, m, r in zip(solved, moved, rounded)]
    rest = [eye - s - mm3(a, s) for a, s in zip(mutuals, solved)]
    return [s + mm(s.astype(bf16), r.astype(bf16)) for s, r in zip(solved, rest)]


def layer_kernel(
    zn,
    resid, query, key, value, fading, step_size, switch, bias, surplus, head_gain, row_gain,
    wo, wg, wu, wd,
    out,
    wo_v, gbuf, ubuf, dbuf,
    solved_s, reach_r, reach_v, reads_s, map_s, add_s, read_map, read_add,
    own_sum, sum_out, sum_in, pair_sum, state_out, state_in, entering,
    mixed, part, kept, core_out, core_in, y_out, y_in, z_out, z_in,
    middle, tokens, hidden,
    local_sem, wz_s, wz_r, wx_s, wx_r, sum_sem, state_sem,
    core_s, core_r, y_s, y_r, z_s, z_r,
    own_s, ring_s, ring_r, ty_s, ty_r, tc_s, tc_r, td_s, td_r,
):
    sp, tp = lax.axis_index("sp"), lax.axis_index("tp")
    z, x = sp // PAIR, sp % PAIR
    t_core = tp + 1 - 2 * (tp % 2)
    t_y = (tp + 2) % 4
    t_both = (t_core + 2) % 4
    rows, width = resid.shape
    positions = query.shape[1]
    blocks = positions // LANES
    pairs = query.shape[0] // LANES
    depth = wg.shape[0]
    taken = gbuf.shape[1] // LANES
    tiles = wg.shape[1] // LANES
    bits = (zn - 1).bit_length()

    def zx(g):
        return sum(((z // (1 << i) + (g >> i)) % 2) * (1 << i) for i in range(bits))

    def at(zz, xx, tt):
        return {"sp": zz * PAIR + xx, "tp": tt}

    def first_tile(zz):
        return (zz * (tiles - taken)) // (zn - 1)

    def remote(src, dst, send, recv, to):
        return pltpu.make_async_remote_copy(
            src_ref=src, dst_ref=dst, send_sem=send, recv_sem=recv, device_id=to, device_id_type=MESH
        )

    x_peer, y_peer, core_peer = at(z, 1 - x, tp), at(z, x, t_y), at(z, x, t_core)

    barrier = pltpu.get_barrier_semaphore()
    peers = [x_peer, y_peer, core_peer] + [at(zx(g), x, tp) for g in range(1, zn)]
    for peer in peers:
        pl.semaphore_signal(barrier, inc=1, device_id=peer, device_id_type=MESH)
    pl.semaphore_wait(barrier, len(peers))

    def wide(ref, zz):
        return ref.at[:, pl.ds(pl.multiple_of(first_tile(zz) * LANES, LANES), taken * LANES)]

    def tall(ref, zz):
        return ref.at[pl.ds(pl.multiple_of(first_tile(zz) * LANES, LANES), taken * LANES), :]

    def slots(place):
        span = pl.ds(pl.multiple_of(place * depth, depth), depth)
        return gbuf.at[span, :], ubuf.at[span, :], dbuf.at[:, span]

    def cut(zz):
        return wide(wg, zz), wide(wu, zz), tall(wd, zz)

    own_copies = [pltpu.make_async_copy(wo, wo_v, local_sem.at[3])] + [
        pltpu.make_async_copy(a, b, local_sem.at[i])
        for i, (a, b) in enumerate(zip(cut(z), slots(sp)))
    ]

    def z_weights(g):
        return [
            remote(a, b, wz_s.at[g, i], wz_r.at[g, i], at(zx(g), x, tp))
            for i, (a, b) in enumerate(zip(cut(zx(g)), slots(sp)))
        ]

    def x_weights(g):
        there = slots(zx(g) * PAIR + x)
        return [
            remote(a, b, wx_s.at[g, i], wx_r.at[g, i], x_peer)
            for i, (a, b) in enumerate(zip(cut(z) if g == 0 else there, there))
        ]

    def start(copies):
        for c in copies:
            c.start()

    def forward(g):
        for c, onward in zip(z_weights(g), x_weights(g)):
            c.wait_recv()
            onward.start()

    far_first = list(range(zn - 1, 0, -1))
    start(own_copies)
    start(x_weights(0))
    start(z_weights(far_first[0]))

    row, col = grid_of(LANES)
    strict, up_to = row < col, row <= col
    row_h, col_h = grid_of(HEAD)
    left = col_h < HEAD

    def first_part(hp, _):
        r0 = pl.multiple_of(hp * LANES, LANES)
        here = pl.ds(r0, LANES)
        keys = key[here, :].astype(f32)
        extra = jnp.concatenate(
            [
                jnp.broadcast_to(surplus[pl.ds(2 * hp + i, 1), :], (HEAD, positions))
                for i in range(2)
            ],
            axis=0,
        )
        pre = fading[here, :].astype(f32) + bias[here, :]
        log_fade = -0.6065306597126334 / (1.0 + jnp.exp(-pre)) + extra
        rate = 1.0 / (1.0 + jnp.exp(-step_size[here, :].astype(f32)))
        unit = jnp.concatenate(
            [
                h * lax.rsqrt(jnp.sum(h * h, axis=0, keepdims=True) + key_eps)
                for h in (keys[:HEAD], keys[HEAD:])
            ],
            axis=0,
        )
        removal, scaled = unit * rate, keys * rate
        reads = query[here, :].astype(f32)
        values = value[here, :]
        ones = jnp.where(up_to, 1.0, 0.0).astype(bf16)
        mutuals, grams, ends, probes = [], [], [], []
        for b in range(blocks):
            lanes = slice(b * LANES, (b + 1) * LANES)
            fade = log_fade[:, lanes]
            f1 = fade.astype(bf16)
            left_over = fade - f1.astype(f32)
            f2 = left_over.astype(bf16)
            f3 = (left_over - f2.astype(f32)).astype(bf16)
            after = mm(f1, ones) + (mm(f2, ones) + mm(f3, ones))
            before = after - fade
            mid, last = after[:, HEAD - 1 : HEAD], after[:, LANES - 1 :]
            shrink = jnp.exp(mid - after)
            probe = unit[:, lanes] * jnp.exp(before - mid)
            read = reads[:, lanes] * jnp.exp(after - mid)
            removal_in, scaled_in = removal[:, lanes] * shrink, scaled[:, lanes] * shrink
            to_mid, to_end = jnp.exp(mid), jnp.exp(last - mid)
            reads_s[hp * blocks + b] = read * to_mid
            probes.append(probe * to_mid)
            ends.append((removal_in * to_end, scaled_in * to_end, jnp.exp(last)))
            none = jnp.zeros((HEAD, LANES), f32)
            for hh in range(2):
                own = slice(hh * HEAD, (hh + 1) * HEAD)
                turned = jnp.concatenate([removal_in[own], scaled_in[own]], axis=0).T
                right = jnp.concatenate(
                    [
                        jnp.concatenate([probe[own], read[own], none, none], axis=1),
                        jnp.concatenate([none, none, probe[own], read[own]], axis=1),
                    ],
                    axis=0,
                )
                gram = mm3(turned, right)
                mutuals.append(jnp.where(strict, gram[:, :LANES], 0.0))
                place = (hp * blocks + b) * 2 + hh
                reach_r[place] = jnp.where(up_to, gram[:, LANES : 2 * LANES], 0.0)
                reach_v[place] = jnp.where(up_to, gram[:, 3 * LANES :], 0.0)
                grams.append(jnp.where(strict, gram[:, 2 * LANES : 3 * LANES], 0.0))
        inverse = inverses(mutuals)
        total = None
        for b in range(blocks):
            lanes = slice(b * LANES, (b + 1) * LANES)
            removal_end, scaled_end, fade_end = ends[b]
            taken_out, added = [], []
            for hh in range(2):
                own = slice(hh * HEAD, (hh + 1) * HEAD)
                vals = values[own, lanes]
                right = jnp.concatenate([probes[b][own], mm2(vals, grams[b * 2 + hh])], axis=0)
                solved = mm3(right, inverse[b * 2 + hh])
                solved_s[(hp * blocks + b) * 2 + hh] = solved
                taken_out.append(mm3(solved, removal_end, NT))
                added.append(mm2(vals, scaled_end, NT))
            both = [jnp.where(left, taken_out[0][i], taken_out[1][i]) for i in (slice(0, HEAD), slice(HEAD, LANES))]
            fade_both = jnp.where(left, fade_end[:HEAD], fade_end[HEAD:])
            carry_map = jnp.where(row_h == col_h % HEAD, fade_both, 0.0) - both[0]
            carry_add = jnp.where(left, added[0], added[1]) - both[1]
            map_s[hp * blocks + b] = carry_map
            add_s[hp * blocks + b] = carry_add
            if total is None:
                total = jnp.concatenate([carry_map, carry_add], axis=0)
            else:
                total = mm3(total, heads_apart(carry_map)) + jnp.concatenate(
                    [jnp.zeros_like(carry_add), carry_add], axis=0
                )
        own_sum[hp] = total
        sum_out[hp] = total.astype(bf16)
        return _

    lax.fori_loop(0, pairs, first_part, 0)

    sum_copy = remote(sum_out, sum_in, sum_sem.at[0], sum_sem.at[1], x_peer)
    sum_copy.start()

    def reading_part(hp, _):
        here = pl.ds(pl.multiple_of(hp * LANES, LANES), LANES)
        for b in range(blocks):
            lanes = slice(b * LANES, (b + 1) * LANES)
            maps, adds = [], []
            reads = reads_s[hp * blocks + b]
            values = value[here, lanes]
            for hh in range(2):
                own = slice(hh * HEAD, (hh + 1) * HEAD)
                place = (hp * blocks + b) * 2 + hh
                gone = mm3(solved_s[place], reach_r[place])
                maps.append(reads[own] - gone[:HEAD])
                adds.append(mm2(values[own], reach_v[place]) - gone[HEAD:])
            read_map[hp * blocks + b] = jnp.concatenate(maps, axis=0)
            read_add[hp * blocks + b] = jnp.concatenate(adds, axis=0)
        return _

    lax.fori_loop(0, pairs, reading_part, 0)
    sum_copy.wait_recv()

    def pair_part(hp, _):
        got, own = sum_in[hp].astype(f32), own_sum[hp]
        first = jnp.where(x == 0, own, got)
        second = jnp.where(x == 0, got, own)
        pair_sum[hp] = mm3(first, heads_apart(second[:HEAD])) + jnp.concatenate(
            [jnp.zeros((HEAD, LANES), f32), second[HEAD:]], axis=0
        )
        return _

    lax.fori_loop(0, pairs, pair_part, 0)

    up_z, down_z = (z + 1) % zn, (z + zn - 1) % zn
    state_copy = remote(state_out, state_in, state_sem.at[0], state_sem.at[1], at(up_z, x, tp))

    @pl.when(z == 0)
    def _():
        state_in[...] = jnp.zeros_like(state_in)

    @pl.when(z > 0)
    def _():
        state_copy.wait_recv()

    def chain_part(hp, _):
        state_out[hp] = (
            mm2(state_in[hp], heads_apart(pair_sum[hp, :HEAD])) + pair_sum[hp, HEAD:]
        ).astype(bf16)
        return _

    lax.fori_loop(0, pairs, chain_part, 0)

    @pl.when(z < zn - 1)
    def _():
        state_copy.start()

    for g in far_first[1:]:
        start(z_weights(g))

    def second_part(hp, _):
        r0 = pl.multiple_of(hp * LANES, LANES)
        here = pl.ds(r0, LANES)
        came = state_in[hp].astype(f32)
        got = sum_in[hp].astype(f32)
        state = jnp.where(x == 0, came, mm3(came, heads_apart(got[:HEAD])) + got[HEAD:])
        for b in range(blocks):
            place = hp * blocks + b
            result = mm3(heads_apart(state), read_map[place]) + read_add[place]
            normed = []
            for h in (result[:HEAD], result[HEAD:]):
                centred = h - jnp.mean(h, axis=0, keepdims=True)
                normed.append(
                    centred * lax.rsqrt(jnp.mean(centred * centred, axis=0, keepdims=True) + group_eps)
                )
            lanes = slice(b * LANES, (b + 1) * LANES)
            done = jnp.concatenate(normed, axis=0) * head_gain[here, :] * switch[here, lanes].astype(f32)
            mixed[lanes, here] = done.T.astype(bf16)
            if b + 1 < blocks:
                state = mm3(state, heads_apart(map_s[place])) + add_s[place]
        return _

    lax.fori_loop(0, pairs, second_part, 0)

    step = 4 * LANES
    own_copies[0].wait()

    def project(i, _):
        cols = pl.ds(pl.multiple_of(i * step, step), step)
        part[0, :, cols] = mm(mixed[...], wo_v[:, cols])
        return _

    lax.fori_loop(0, width // step, project, 0)

    def rows_for(t):
        return pl.ds(pl.multiple_of(t * rows, rows), rows)

    def core_copy(i):
        return remote(core_out.at[i], core_in.at[i], core_s.at[i], core_r.at[i], core_peer)

    def y_copy(i):
        return remote(y_out.at[i], y_in.at[i], y_s.at[i], y_r.at[i], y_peer)

    def send_core(i, buf):
        core_out[i, 0] = part[buf, rows_for(t_core), :].astype(bf16)
        core_out[i, 1] = part[buf, rows_for(t_both), :].astype(bf16)
        core_copy(i).start()

    def send_y(i, buf):
        core_copy(i).wait_recv()
        y_out[i] = (part[buf, rows_for(t_y), :] + core_in[i, 1].astype(f32)).astype(bf16)
        y_copy(i).start()
        kept[i] = part[buf, rows_for(tp), :] + core_in[i, 0].astype(f32)

    send_core(zn, 0)
    send_y(zn, 0)
    forward(far_first[0])
    y_copy(zn).wait_recv()
    middle[...] = resid[...].astype(f32) + (kept[zn] + y_in[zn].astype(f32))
    mid_rows = middle[...]
    scale = lax.rsqrt(jnp.mean(mid_rows * mid_rows, axis=-1, keepdims=True) + norm_eps)
    tokens[z, rows_for(tp), :] = (mid_rows * scale * row_gain[...]).astype(bf16)

    def piece(zz, t):
        return tokens.at[zz, rows_for(t), :]

    def up_copy(zz, sem):
        return remote(piece(zz, tp), piece(zz, tp), sem, ring_r.at[zz], at(up_z, x, tp))

    def down_copy(zz, sem):
        return remote(piece(zz, tp), piece(zz, tp), sem, ring_r.at[zz], at(down_z, x, tp))

    def when(cond, action):
        pl.when(cond)(action)

    def y_token(g):
        return remote(piece(zx(g), tp), piece(zx(g), tp), ty_s.at[g], ty_r.at[g], y_peer)

    def y_token_came(g):
        return remote(piece(zx(g), t_y), piece(zx(g), t_y), ty_s.at[g], ty_r.at[g], y_peer)

    def core_token(g):
        return remote(piece(zx(g), tp), piece(zx(g), tp), tc_s.at[g], tc_r.at[g], core_peer)

    def core_token_came(g):
        return remote(piece(zx(g), t_core), piece(zx(g), t_core), tc_s.at[g], tc_r.at[g], core_peer)

    def both_token(g):
        return remote(piece(zx(g), t_y), piece(zx(g), t_y), td_s.at[g], td_r.at[g], core_peer)

    def both_token_came(g):
        return remote(piece(zx(g), t_both), piece(zx(g), t_both), td_s.at[g], td_r.at[g], core_peer)

    def spread_z(g):
        zz = zx(g)
        if g == 0:
            when(z < zn - 1, lambda: up_copy(zz, own_s.at[0]).start())
            when(z > 0, lambda: down_copy(zz, own_s.at[1]).start())
        else:
            up_copy(zz, ring_s.at[g]).wait_recv()
            when((zz < z) & (z < zn - 1), lambda: up_copy(zz, ring_s.at[g]).start())
            when((zz > z) & (z > 0), lambda: down_copy(zz, ring_s.at[g]).start())
        y_token(g).start()
        core_token(g).start()

    def spread_y(g):
        y_token_came(g).wait_recv()
        both_token(g).start()

    spread_z(0)
    spread_y(0)
    for g in far_first[1:]:
        forward(g)
    for g in range(1, zn):
        spread_z(g)
        spread_y(g)
    for c in own_copies[1:]:
        c.wait()
    for g in range(zn):
        for c in x_weights(g):
            c.wait_recv()

    unit_at = lax.broadcasted_iota(jnp.int32, (1, taken * LANES), 1)
    mine = unit_at >= jnp.where(z == 0, 0, (first_tile(z - 1) + taken - first_tile(z)) * LANES)

    def feed(g, buf):
        core_token_came(g).wait_recv()
        both_token_came(g).wait_recv()
        block = tokens[zx(g)]
        gate = mm(block, gbuf[...])
        up = mm(block, ubuf[...])
        hidden[...] = jnp.where(mine, gate / (1.0 + jnp.exp(-gate)) * up, 0.0).astype(bf16)

        def down(i, _):
            cols = pl.ds(pl.multiple_of(i * step, step), step)
            part[buf, :, cols] = mm(hidden[...], dbuf[:, cols])
            return _

        lax.fori_loop(0, width // step, down, 0)

    def z_copy(g):
        return remote(z_out.at[g], z_in.at[g], z_s.at[g], z_r.at[g], at(zx(g), x, tp))

    def send_z(g):
        y_copy(g).wait_recv()
        if g == 0:
            kept[g] = kept[g] + y_in[g].astype(f32)
        else:
            z_out[g] = (kept[g] + y_in[g].astype(f32)).astype(bf16)
            z_copy(g).start()

    order = list(range(1, zn)) + [0]
    for i, g in enumerate(order):
        feed(g, i % 2)
        send_core(g, i % 2)
        if i >= 1:
            send_y(order[i - 1], (i - 1) % 2)
        if i >= 2:
            send_z(order[i - 2])
    send_y(order[-1], (zn - 1) % 2)
    send_z(order[-2])
    send_z(order[-1])
    total = middle[...] + kept[0]
    for g in range(1, zn):
        z_copy(g).wait_recv()
        total = total + z_in[g].astype(f32)
    out[...] = total.astype(bf16)

    for g in range(1, zn):
        for c in z_weights(g):
            c.wait_send()
        z_copy(g).wait_send()
        zz = zx(g)
        moved_on = ((zz < z) & (z < zn - 1)) | ((zz > z) & (z > 0))
        when(moved_on, up_copy(zz, ring_s.at[g]).wait_send)
    for g in range(zn):
        for c in x_weights(g):
            c.wait_send()
        y_token(g).wait_send()
        core_token(g).wait_send()
        both_token(g).wait_send()
    for i in range(zn + 1):
        core_copy(i).wait_send()
        y_copy(i).wait_send()
    sum_copy.wait_send()
    when(z < zn - 1, state_copy.wait_send)
    when(z < zn - 1, up_copy(z, own_s.at[0]).wait_send)
    when(z > 0, down_copy(z, own_s.at[1]).wait_send)


def fits(mesh, *arrays):
    sp, tp = mesh.shape["sp"], mesh.shape["tp"]
    heads, positions = arrays[8].shape
    units = arrays[12].shape[1]
    zn = sp // PAIR
    return (
        tp == 4
        and sp % PAIR == 0
        and zn > 1
        and zn & (zn - 1) == 0
        and heads % 2 == 0
        and positions % LANES == 0
        and positions == tp * arrays[0].shape[0]
        and units % LANES == 0
        and units // LANES >= zn
        and arrays[12].shape[0] % LANES == 0
        and arrays[0].shape[1] % (4 * LANES) == 0
    )


def fused(
    residual, query, key, value, fading, step_size, switch, bias, surplus, head_gain, out_proj,
    row_gain, gate_up, expand, contract,
):
    zn = lax.axis_size("sp") // PAIR
    rows, width = residual.shape
    channels, positions = query.shape
    pairs, blocks = channels // LANES, positions // LANES
    many = pairs * blocks
    taken = -(-(gate_up.shape[1] // LANES) // zn) * LANES
    square = (LANES, LANES)
    half = (HEAD, LANES)
    vmem, dma = pltpu.VMEM, pltpu.SemaphoreType.DMA
    scratch = [
        vmem(out_proj.shape, bf16),
        vmem((width, taken), bf16),
        vmem((width, taken), bf16),
        vmem((taken, width), bf16),
        vmem((2 * many, *square), f32),
        vmem((2 * many, *square), f32),
        vmem((2 * many, *square), f32),
        vmem((many, *square), f32),
        vmem((many, *half), f32),
        vmem((many, *half), f32),
        vmem((many, *square), f32),
        vmem((many, *square), f32),
        vmem((pairs, *square), f32),
        vmem((pairs, *square), bf16),
        vmem((pairs, *square), bf16),
        vmem((pairs, *square), f32),
        vmem((pairs, *half), bf16),
        vmem((pairs, *half), bf16),
        vmem((pairs, *half), f32),
        vmem((positions, channels), bf16),
        vmem((2, positions, width), f32),
        vmem((zn + 1, rows, width), f32),
        vmem((zn + 1, 2, rows, width), bf16),
        vmem((zn + 1, 2, rows, width), bf16),
        vmem((zn + 1, rows, width), bf16),
        vmem((zn + 1, rows, width), bf16),
        vmem((zn, rows, width), bf16),
        vmem((zn, rows, width), bf16),
        vmem((rows, width), f32),
        vmem((zn, positions, width), bf16),
        vmem((positions, taken), bf16),
        dma((4,)),
        dma((zn, 3)), dma((zn, 3)), dma((zn, 3)), dma((zn, 3)),
        dma((2,)), dma((2,)),
        dma((zn + 1,)), dma((zn + 1,)), dma((zn + 1,)), dma((zn + 1,)), dma((zn,)), dma((zn,)),
        dma((2,)), dma((zn,)), dma((zn,)),
        dma((zn,)), dma((zn,)), dma((zn,)), dma((zn,)), dma((zn,)), dma((zn,)),
    ]
    inside = pl.BlockSpec(memory_space=pltpu.VMEM)
    outside = pl.BlockSpec(memory_space=pl.ANY)
    return pl.pallas_call(
        functools.partial(layer_kernel, zn),
        out_shape=jax.ShapeDtypeStruct((rows, width), bf16),
        in_specs=[inside] * 11 + [outside] * 4,
        out_specs=inside,
        scratch_shapes=scratch,
        compiler_params=pltpu.CompilerParams(
            collective_id=0, has_side_effects=True, vmem_limit_bytes=60 << 20
        ),
        name="layer",
    )(
        residual, query, key, value, fading, step_size, switch, bias[:, None], surplus,
        head_gain[:, None], row_gain[None, :], out_proj, gate_up, expand, contract,
    )


def solution(mesh):
    placed = (
        P(("sp", "tp"), None),
        P("tp", "sp"),
        P("tp", "sp"),
        P("tp", "sp"),
        P("tp", "sp"),
        P("tp", "sp"),
        P("tp", "sp"),
        P("tp"),
        P("tp", "sp"),
        P("tp"),
        P("tp", None),
        P(),
        P("sp", "tp"),
        P("sp", "tp"),
        P("tp", "sp"),
    )

    def layer(*arrays):
        return (fused if fits(mesh, *arrays) else local)(*arrays)


    return jax.shard_map(
        layer, mesh=mesh, in_specs=placed, out_specs=P(("sp", "tp"), None), check_vma=False
    )
```

profile of v0, /device:TPU:0, one launch (start us, length us, event | category | flops | bytes accessed | tf_op | source)
XLA Modules:
  0.0 164.3 jit_solution(16947148234966735928)
XLA Ops:
  0.0 1.5 copy.16.bias
  1.5 1.5 copy.17.head_gain
  3.1 159.6 %layer.1 = bf16[64,2048]{1,0:T(8,128)(2,1)} custom-call(bf16[64,2048]{1,0:T(8,128)(2,1)} %resid.1, bf16[512,256]{1,0:T(8,128)(2,1)} %query.1, bf16[512,256]{1,0:T(8,128)(2,1)} %key.1, bf16[512,256]{1,0:T(8,128)(2,1)} %value.1, bf16[512,256]{1,0:T(8,128)(2,1)} %fading.1, bf16[512,256]{1,0:T(8,128)(2,1)} %step_size.1, bf16[512,256]{1,0:T(8,128)(2,1)} %switch.1, ...), custom_call_target="tpu_custom_call" | custom-call | tf_op jit(solution)/shard_map/layer/pallas_call | solution.py:857
  162.6 1.7 %copy.19 = bf16[64,2048]{1,0:T(8,128)(2,1)} copy(bf16[64,2048]{1,0:T(8,128)(2,1)} %layer.1) | data formatting | bytes 524288
where the time goes:
time: 165 us; the launch traced here: 164 us
  Pallas kernels  160 us (97%)
  local copies, waits for them, and re-layouts  4.73 us (3%)
    pallas_call x1, Pallas kernels, fused(): pl.pallas_call(functools.partial(layer_kernel, zn), out_shape=jax.ShapeDt...  160 us

commit v1 on v0

--- a/solution.py
+++ b/solution.py
@@ -365,8 +365,13 @@
     tiles = wg.shape[1] // LANES
     bits = (zn - 1).bit_length()
 
+    own_group = 0
+
+    def is_own(g):
+        return isinstance(g, int) and g == own_group
+
     def zx(g):
-        return sum(((z // (1 << i) + (g >> i)) % 2) * (1 << i) for i in range(bits))
+        return sum(((z // (1 << i) + g // (1 << i)) % 2) * (1 << i) for i in range(bits))
 
     def at(zz, xx, tt):
         return {"sp": zz * PAIR + xx, "tp": tt}
@@ -415,29 +420,51 @@
         there = slots(zx(g) * PAIR + x)
         return [
             remote(a, b, wx_s.at[g, i], wx_r.at[g, i], x_peer)
-            for i, (a, b) in enumerate(zip(cut(z) if g == 0 else there, there))
+            for i, (a, b) in enumerate(zip(cut(z) if is_own(g) else there, there))
         ]
+
+    def column(ref, hp):
+        return jnp.broadcast_to(ref[pl.ds(hp, 1), :], (LANES, LANES)).T
 
     def start(copies):
         for c in copies:
             c.start()
 
-    def forward(g):
-        for c, onward in zip(z_weights(g), x_weights(g)):
+    def start_up(g, which):
+        pl.when(zx(g) > z)(lambda: start(z_weights(g)[which]))
+
+    def start_down(g, which):
+        pl.when(zx(g) < z)(lambda: start(z_weights(g)[which]))
+
+    def forward(g, which):
+        for c, onward in zip(z_weights(g)[which], x_weights(g)[which]):
             c.wait_recv()
             onward.start()
+
+    inner = ((z + 1) // 2) % 2
+    tail = list(range(4, zn))
+    arrive = [3 - inner, 1 + 2 * inner, 2 - inner] + tail if zn >= 4 else [1]
+    pieces = [1, 2 + inner, 3 - inner] + tail if zn >= 4 else [1]
+    every, wide_two, tall_one = slice(0, 3), slice(0, 2), slice(2, 3)
 
     far_first = list(range(zn - 1, 0, -1))
     start(own_copies)
     start(x_weights(0))
-    start(z_weights(far_first[0]))
+    for g in far_first:
+        start_down(g, every)
+
+    @pl.when(z == 0)
+    def _():
+        for g in far_first[:-1]:
+            start(z_weights(g)[every if g > 2 else wide_two])
+
 
     row, col = grid_of(LANES)
     strict, up_to = row < col, row <= col
     row_h, col_h = grid_of(HEAD)
     left = col_h < HEAD
 
-    def first_part(hp, _):
+    def prepared(hp, mutuals, grams):
         r0 = pl.multiple_of(hp * LANES, LANES)
         here = pl.ds(r0, LANES)
         keys = key[here, :].astype(f32)
@@ -448,7 +475,7 @@
             ],
             axis=0,
         )
-        pre = fading[here, :].astype(f32) + bias[here, :]
+        pre = fading[here, :].astype(f32) + jnp.tile(column(bias, hp), (1, blocks))
         log_fade = -0.6065306597126334 / (1.0 + jnp.exp(-pre)) + extra
         rate = 1.0 / (1.0 + jnp.exp(-step_size[here, :].astype(f32)))
         unit = jnp.concatenate(
@@ -460,9 +487,8 @@
         )
         removal, scaled = unit * rate, keys * rate
         reads = query[here, :].astype(f32)
-        values = value[here, :]
         ones = jnp.where(up_to, 1.0, 0.0).astype(bf16)
-        mutuals, grams, ends, probes = [], [], [], []
+        ends, probes = [], []
         for b in range(blocks):
             lanes = slice(b * LANES, (b + 1) * LANES)
             fade = log_fade[:, lanes]
@@ -498,7 +524,10 @@
                 reach_r[place] = jnp.where(up_to, gram[:, LANES : 2 * LANES], 0.0)
                 reach_v[place] = jnp.where(up_to, gram[:, 3 * LANES :], 0.0)
                 grams.append(jnp.where(strict, gram[:, 2 * LANES : 3 * LANES], 0.0))
-        inverse = inverses(mutuals)
+        return ends, probes
+
+    def summed(hp, ends, probes, inverse, grams):
+        values = value[pl.ds(pl.multiple_of(hp * LANES, LANES), LANES), :]
         total = None
         for b in range(blocks):
             lanes = slice(b * LANES, (b + 1) * LANES)
@@ -512,7 +541,10 @@
                 solved_s[(hp * blocks + b) * 2 + hh] = solved
                 taken_out.append(mm3(solved, removal_end, NT))
                 added.append(mm2(vals, scaled_end, NT))
-            both = [jnp.where(left, taken_out[0][i], taken_out[1][i]) for i in (slice(0, HEAD), slice(HEAD, LANES))]
+            both = [
+                jnp.where(left, taken_out[0][i], taken_out[1][i])
+                for i in (slice(0, HEAD), slice(HEAD, LANES))
+            ]
             fade_both = jnp.where(left, fade_end[:HEAD], fade_end[HEAD:])
             carry_map = jnp.where(row_h == col_h % HEAD, fade_both, 0.0) - both[0]
             carry_add = jnp.where(left, added[0], added[1]) - both[1]
@@ -526,9 +558,20 @@
                 )
         own_sum[hp] = total
         sum_out[hp] = total.astype(bf16)
+
+    together = 2 if pairs % 2 == 0 else 1
+
+    def first_part(i, _):
+        mutuals, grams, ready = [], [], []
+        for j in range(together):
+            ready.append(prepared(i * together + j, mutuals, grams))
+        inverse = inverses(mutuals)
+        for j in range(together):
+            span = slice(j * 2 * blocks, (j + 1) * 2 * blocks)
+            summed(i * together + j, *ready[j], inverse[span], grams[span])
         return _
 
-    lax.fori_loop(0, pairs, first_part, 0)
+    lax.fori_loop(0, pairs // together, first_part, 0)
 
     sum_copy = remote(sum_out, sum_in, sum_sem.at[0], sum_sem.at[1], x_peer)
     sum_copy.start()
@@ -587,13 +630,23 @@
     def _():
         state_copy.start()
 
-    for g in far_first[1:]:
-        start(z_weights(g))
+    @pl.when(z == 0)
+    def _():
+        start(z_weights(1)[wide_two])
+        if zn > 2:
+            start(z_weights(2)[tall_one])
+
+    @pl.when(z > 0)
+    def _():
+        for g in [1] + far_first[:-1]:
+            start_up(g, every)
+
 
     def second_part(hp, _):
         r0 = pl.multiple_of(hp * LANES, LANES)
         here = pl.ds(r0, LANES)
         came = state_in[hp].astype(f32)
+        gain = column(head_gain, hp)
         got = sum_in[hp].astype(f32)
         state = jnp.where(x == 0, came, mm3(came, heads_apart(got[:HEAD])) + got[HEAD:])
         for b in range(blocks):
@@ -606,7 +659,7 @@
                     centred * lax.rsqrt(jnp.mean(centred * centred, axis=0, keepdims=True) + group_eps)
                 )
             lanes = slice(b * LANES, (b + 1) * LANES)
-            done = jnp.concatenate(normed, axis=0) * head_gain[here, :] * switch[here, lanes].astype(f32)
+            done = jnp.concatenate(normed, axis=0) * gain * switch[here, lanes].astype(f32)
             mixed[lanes, here] = done.T.astype(bf16)
             if b + 1 < blocks:
                 state = mm3(state, heads_apart(map_s[place])) + add_s[place]
@@ -646,7 +699,7 @@
 
     send_core(zn, 0)
     send_y(zn, 0)
-    forward(far_first[0])
+    forward(arrive[0], wide_two)
     y_copy(zn).wait_recv()
     middle[...] = resid[...].astype(f32) + (kept[zn] + y_in[zn].astype(f32))
     mid_rows = middle[...]
@@ -685,7 +738,7 @@
 
     def spread_z(g):
         zz = zx(g)
-        if g == 0:
+        if is_own(g):
             when(z < zn - 1, lambda: up_copy(zz, own_s.at[0]).start())
             when(z > 0, lambda: down_copy(zz, own_s.at[1]).start())
         else:
@@ -699,13 +752,19 @@
         y_token_came(g).wait_recv()
         both_token(g).start()
 
-    spread_z(0)
+    spread_z(own_group)
+    pl.when(z == 0)(lambda: start(z_weights(1)[tall_one]))
+    forward(arrive[0], tall_one)
+    if zn > 2:
+        forward(arrive[1], every)
     spread_y(0)
-    for g in far_first[1:]:
-        forward(g)
-    for g in range(1, zn):
+    for g in arrive[2:]:
+        forward(g, every)
+    for i, g in enumerate(pieces):
         spread_z(g)
-        spread_y(g)
+        if i > 0:
+            spread_y(pieces[i - 1])
+    spread_y(pieces[-1])
     for c in own_copies[1:]:
         c.wait()
     for g in range(zn):
@@ -735,13 +794,13 @@
 
     def send_z(g):
         y_copy(g).wait_recv()
-        if g == 0:
+        if is_own(g):
             kept[g] = kept[g] + y_in[g].astype(f32)
         else:
             z_out[g] = (kept[g] + y_in[g].astype(f32)).astype(bf16)
             z_copy(g).start()
 
-    order = list(range(1, zn)) + [0]
+    order = pieces[1:] + pieces[:1] + [own_group]
     for i, g in enumerate(order):
         feed(g, i % 2)
         send_core(g, i % 2)
@@ -865,8 +924,8 @@
         ),
         name="layer",
     )(
-        residual, query, key, value, fading, step_size, switch, bias[:, None], surplus,
-        head_gain[:, None], row_gain[None, :], out_proj, gate_up, expand, contract,
+        residual, query, key, value, fading, step_size, switch, bias.reshape(pairs, LANES), surplus,
+        head_gain.reshape(pairs, LANES), row_gain[None, :], out_proj, gate_up, expand, contract,
     )
 
 

time: 165 us -> 124 us (0.75)
  Pallas kernels: 160 us -> 122 us
  local copies, waits for them, and re-layouts: 4.73 us -> 1.67 us
    pallas_call x1, Pallas kernels: 160 us -> 122 us  [fused(): pl.pallas_call(functools.partial(layer_kernel, zn), out_shape=jax.ShapeDt...]
    broadcast_in_dim x2 -> x0, local copies, waits for them, and re-layouts: 3.06 us -> none  [the longest x1 1.53 us: fused(): bias[:, None]]
where the time goes in v1:
time: 124 us
  Pallas kernels  122 us (98%)
  local copies, waits for them, and re-layouts  1.67 us (1%)
    pallas_call x1, Pallas kernels, fused(): pl.pallas_call(functools.partial(layer_kernel, zn), out_shape=jax.ShapeDt...  122 us

profile of v1, /device:TPU:0, one launch (start us, length us, event | category | flops | bytes accessed | tf_op | source)
XLA Modules:
  0.0 124.0 jit_solution(2164490441668042535)
XLA Ops:
  0.0 122.3 %layer.1 = bf16[64,2048]{1,0:T(8,128)(2,1)} custom-call(bf16[64,2048]{1,0:T(8,128)(2,1)} %resid.1, bf16[512,256]{1,0:T(8,128)(2,1)} %query.1, bf16[512,256]{1,0:T(8,128)(2,1)} %key.1, bf16[512,256]{1,0:T(8,128)(2,1)} %value.1, bf16[512,256]{1,0:T(8,128)(2,1)} %fading.1, bf16[512,256]{1,0:T(8,128)(2,1)} %step_size.1, bf16[512,256]{1,0:T(8,128)(2,1)} %switch.1, ...), custom_call_target="tpu_custom_call" | custom-call | tf_op jit(solution)/shard_map/layer/pallas_call | solution.py:916
  122.3 1.7 %copy.17 = bf16[64,2048]{1,0:T(8,128)(2,1)} copy(bf16[64,2048]{1,0:T(8,128)(2,1)} %layer.1) | data formatting | bytes 524288

commit v2 on v1

--- a/solution.py
+++ b/solution.py
@@ -283,6 +283,7 @@
 
 LANES = 128
 PAIR = 2
+CUTS = 4
 MESH = pl.DeviceIdType.MESH
 f32, bf16 = jnp.float32, jnp.bfloat16
 NN = (((1,), (0,)), ((), ()))
@@ -300,12 +301,17 @@
 
 def mm3(a, b, dims=NN):
     (ah, al), (bh, bl) = split(a), split(b)
-    return mm(ah, bh, dims) + mm(ah, bl, dims) + mm(al, bh, dims)
+    axis = dims[0][1][0]
+    return mm(
+        jnp.concatenate([ah, al], axis=1), jnp.concatenate([bh, bh], axis=axis), dims
+    ) + mm(ah, bl, dims)
 
 
 def mm2(a, b, dims=NN):
-    bh, bl = split(b)
-    return mm(a, bh, dims) + mm(a, bl, dims)
+    axis = dims[0][1][0]
+    return mm(
+        jnp.concatenate([a, a], axis=1), jnp.concatenate(split(b), axis=axis), dims
+    )
 
 
 def grid_of(rows):
@@ -347,7 +353,8 @@
     own_sum, sum_out, sum_in, pair_sum, state_out, state_in, entering,
     mixed, part, kept, core_out, core_in, y_out, y_in, z_out, z_in,
     middle, tokens, hidden,
-    local_sem, wz_s, wz_r, wx_s, wx_r, sum_sem, state_sem,
+    pair_out, pair_in, step_in,
+    local_sem, pair_sem, step_r, wz_s, wz_r, wx_s, wx_r, sum_sem, state_sem,
     core_s, core_r, y_s, y_r, z_s, z_r,
     own_s, ring_s, ring_r, ty_s, ty_r, tc_s, tc_r, td_s, td_r,
 ):
@@ -361,8 +368,8 @@
     blocks = positions // LANES
     pairs = query.shape[0] // LANES
     depth = wg.shape[0]
-    taken = gbuf.shape[1] // LANES
     tiles = wg.shape[1] // LANES
+    base, spare = tiles // zn, tiles % zn
     bits = (zn - 1).bit_length()
 
     own_group = 0
@@ -377,7 +384,10 @@
         return {"sp": zz * PAIR + xx, "tp": tt}
 
     def first_tile(zz):
-        return (zz * (tiles - taken)) // (zn - 1)
+        return zz * base + sum((zz + zn - 1 - i) // zn for i in range(spare))
+
+    def longer(zz):
+        return zz < spare
 
     def remote(src, dst, send, recv, to):
         return pltpu.make_async_remote_copy(
@@ -392,20 +402,49 @@
         pl.semaphore_signal(barrier, inc=1, device_id=peer, device_id_type=MESH)
     pl.semaphore_wait(barrier, len(peers))
 
-    def wide(ref, zz):
-        return ref.at[:, pl.ds(pl.multiple_of(first_tile(zz) * LANES, LANES), taken * LANES)]
-
-    def tall(ref, zz):
-        return ref.at[pl.ds(pl.multiple_of(first_tile(zz) * LANES, LANES), taken * LANES), :]
+    runs = [(0, base)] + ([(base, 1)] if spare else [])
+
+    def run_start(zz, run):
+        short = (zz + zn - spare) // zn if run[0] else 0
+        return pl.multiple_of((first_tile(zz) + run[0] - short) * LANES, LANES)
+
+    def wide(ref, zz, run):
+        first = run_start(zz, run)
+        return ref.at[:, pl.ds(first, run[1] * LANES)]
+
+    def tall(ref, zz, run):
+        first = run_start(zz, run)
+        return ref.at[pl.ds(first, run[1] * LANES), :]
 
     def slots(place):
         span = pl.ds(pl.multiple_of(place * depth, depth), depth)
-        return gbuf.at[span, :], ubuf.at[span, :], dbuf.at[:, span]
+        units = [slice(a * LANES, (a + n) * LANES) for a, n in runs]
+        return (
+            [w.at[span, u] for u in units for w in (gbuf, ubuf)]
+            + [dbuf.at[u, span] for u in units]
+        )
 
     def cut(zz):
-        return wide(wg, zz), wide(wu, zz), tall(wd, zz)
-
-    own_copies = [pltpu.make_async_copy(wo, wo_v, local_sem.at[3])] + [
+        return [wide(w, zz, run) for run in runs for w in (wg, wu)] + [
+            tall(wd, zz, run) for run in runs
+        ]
+
+    is_spare = [False, False, True, True, False, True] if spare else [False] * 3
+    count = len(is_spare)
+    every, wide_two, tall_one = range(count), range(count * 2 // 3), range(count * 2 // 3, count)
+
+    def each(copies, which, zz, action):
+        for i in which:
+            if is_spare[i]:
+                pl.when(longer(zz))(functools.partial(action, copies[i]))
+            else:
+                action(copies[i])
+
+    def begin(copies, which, zz):
+        each(copies, which, zz, lambda c: c.start())
+
+    wo_copy = pltpu.make_async_copy(wo, wo_v, local_sem.at[count])
+    own_copies = [
         pltpu.make_async_copy(a, b, local_sem.at[i])
         for i, (a, b) in enumerate(zip(cut(z), slots(sp)))
     ]
@@ -426,38 +465,61 @@
     def column(ref, hp):
         return jnp.broadcast_to(ref[pl.ds(hp, 1), :], (LANES, LANES)).T
 
-    def start(copies):
-        for c in copies:
-            c.start()
+    def column(ref, hp):
+        return jnp.broadcast_to(ref[pl.ds(hp, 1), :], (LANES, LANES)).T
 
     def start_up(g, which):
-        pl.when(zx(g) > z)(lambda: start(z_weights(g)[which]))
+        pl.when(zx(g) > z)(lambda: begin(z_weights(g), which, zx(g)))
 
     def start_down(g, which):
-        pl.when(zx(g) < z)(lambda: start(z_weights(g)[which]))
+        pl.when(zx(g) < z)(lambda: begin(z_weights(g), which, zx(g)))
 
     def forward(g, which):
-        for c, onward in zip(z_weights(g)[which], x_weights(g)[which]):
-            c.wait_recv()
-            onward.start()
+        onward = dict(zip(every, x_weights(g)))
+        came = z_weights(g)
+
+        def move(i):
+            came[i].wait_recv()
+            onward[i].start()
+
+        each(list(every), which, z, move)
 
     inner = ((z + 1) // 2) % 2
-    tail = list(range(4, zn))
-    arrive = [3 - inner, 1 + 2 * inner, 2 - inner] + tail if zn >= 4 else [1]
-    pieces = [1, 2 + inner, 3 - inner] + tail if zn >= 4 else [1]
-    every, wide_two, tall_one = slice(0, 3), slice(0, 2), slice(2, 3)
+    rest = list(range(4, zn))
+    arrive = [3 - inner, 1, 2 + inner] + rest if zn >= 4 else [1]
+    pieces = [1, 2 + inner, 3 - inner] + rest if zn >= 4 else [1]
 
     far_first = list(range(zn - 1, 0, -1))
-    start(own_copies)
-    start(x_weights(0))
-    for g in far_first:
-        start_down(g, every)
+    wo_copy.start()
+    begin(own_copies, every, z)
+    begin(x_weights(0), every, z)
+    if zn >= 4:
+
+        @pl.when(inner == 1)
+        def _():
+            for g in [2, 3, 1] + rest:
+                start_down(g, every)
+
+        @pl.when(inner == 0)
+        def _():
+            for g in far_first:
+                start_down(g, every)
+
+    else:
+        start_down(1, every)
 
     @pl.when(z == 0)
     def _():
         for g in far_first[:-1]:
-            start(z_weights(g)[every if g > 2 else wide_two])
-
+            begin(z_weights(g), every, zx(g))
+
+    if spare:
+
+        @pl.when(z >= spare)
+        def _():
+            gbuf[:, base * LANES :] = jnp.zeros((width, LANES), bf16)
+            ubuf[:, base * LANES :] = jnp.zeros((width, LANES), bf16)
+            dbuf[base * LANES :, :] = jnp.zeros((LANES, width), bf16)
 
     row, col = grid_of(LANES)
     strict, up_to = row < col, row <= col
@@ -507,23 +569,26 @@
             reads_s[hp * blocks + b] = read * to_mid
             probes.append(probe * to_mid)
             ends.append((removal_in * to_end, scaled_in * to_end, jnp.exp(last)))
-            none = jnp.zeros((HEAD, LANES), f32)
+            both_in = [split(removal_in), split(scaled_in)]
+            top, low = split(jnp.concatenate([probe, read], axis=1))
             for hh in range(2):
                 own = slice(hh * HEAD, (hh + 1) * HEAD)
-                turned = jnp.concatenate([removal_in[own], scaled_in[own]], axis=0).T
-                right = jnp.concatenate(
+                turned = jnp.concatenate(
                     [
-                        jnp.concatenate([probe[own], read[own], none, none], axis=1),
-                        jnp.concatenate([none, none, probe[own], read[own]], axis=1),
+                        jnp.concatenate([h[own], l[own]], axis=0).astype(f32).T.astype(bf16)
+                        for h, l in both_in
                     ],
                     axis=0,
                 )
-                gram = mm3(turned, right)
-                mutuals.append(jnp.where(strict, gram[:, :LANES], 0.0))
+                right = jnp.concatenate(
+                    [top[own], top[own], low[own], jnp.zeros_like(low[own])], axis=0
+                )
+                gram = mm(jnp.concatenate([turned, turned], axis=1), right)
+                mutuals.append(jnp.where(strict, gram[:LANES, :LANES], 0.0))
                 place = (hp * blocks + b) * 2 + hh
-                reach_r[place] = jnp.where(up_to, gram[:, LANES : 2 * LANES], 0.0)
-                reach_v[place] = jnp.where(up_to, gram[:, 3 * LANES :], 0.0)
-                grams.append(jnp.where(strict, gram[:, 2 * LANES : 3 * LANES], 0.0))
+                reach_r[place] = jnp.where(up_to, gram[:LANES, LANES:], 0.0)
+                reach_v[place] = jnp.where(up_to, gram[LANES:, LANES:], 0.0)
+                grams.append(jnp.where(strict, gram[LANES:, :LANES], 0.0))
         return ends, probes
 
     def summed(hp, ends, probes, inverse, grams):
@@ -561,6 +626,10 @@
 
     together = 2 if pairs % 2 == 0 else 1
 
+    def sum_copy(i):
+        share = pl.ds(i * together, together)
+        return remote(sum_out.at[share], sum_in.at[share], sum_sem.at[0, i], sum_sem.at[1, i], x_peer)
+
     def first_part(i, _):
         mutuals, grams, ready = [], [], []
         for j in range(together):
@@ -569,12 +638,11 @@
         for j in range(together):
             span = slice(j * 2 * blocks, (j + 1) * 2 * blocks)
             summed(i * together + j, *ready[j], inverse[span], grams[span])
+        sum_copy(i).start()
         return _
 
     lax.fori_loop(0, pairs // together, first_part, 0)
 
-    sum_copy = remote(sum_out, sum_in, sum_sem.at[0], sum_sem.at[1], x_peer)
-    sum_copy.start()
 
     def reading_part(hp, _):
         here = pl.ds(pl.multiple_of(hp * LANES, LANES), LANES)
@@ -594,7 +662,8 @@
         return _
 
     lax.fori_loop(0, pairs, reading_part, 0)
-    sum_copy.wait_recv()
+    for i in range(pairs // together):
+        sum_copy(i).wait_recv()
 
     def pair_part(hp, _):
         got, own = sum_in[hp].astype(f32), own_sum[hp]
@@ -606,6 +675,12 @@
         return _
 
     lax.fori_loop(0, pairs, pair_part, 0)
+    if zn >= 4:
+
+        @pl.when(inner == 0)
+        def _():
+            forward(arrive[0], every)
+
 
     up_z, down_z = (z + 1) % zn, (z + zn - 1) % zn
     state_copy = remote(state_out, state_in, state_sem.at[0], state_sem.at[1], at(up_z, x, tp))
@@ -632,14 +707,26 @@
 
     @pl.when(z == 0)
     def _():
-        start(z_weights(1)[wide_two])
-        if zn > 2:
-            start(z_weights(2)[tall_one])
+        begin(z_weights(1), wide_two, zx(1))
 
     @pl.when(z > 0)
     def _():
-        for g in [1] + far_first[:-1]:
-            start_up(g, every)
+        start_up(1, every)
+        if zn >= 4:
+            start_up(3, wide_two)
+            start_up(2, every)
+            start_up(3, tall_one)
+            for g in rest:
+                start_up(g, every)
+
+    if zn >= 4:
+
+        @pl.when(inner == 1)
+        def _():
+            forward(arrive[0], every)
+
+    else:
+        forward(arrive[0], every)
 
 
     def second_part(hp, _):
@@ -668,7 +755,7 @@
     lax.fori_loop(0, pairs, second_part, 0)
 
     step = 4 * LANES
-    own_copies[0].wait()
+    wo_copy.wait()
 
     def project(i, _):
         cols = pl.ds(pl.multiple_of(i * step, step), step)
@@ -683,8 +770,12 @@
     def core_copy(i):
         return remote(core_out.at[i], core_in.at[i], core_s.at[i], core_r.at[i], core_peer)
 
-    def y_copy(i):
-        return remote(y_out.at[i], y_in.at[i], y_s.at[i], y_r.at[i], y_peer)
+    cuts = [slice(i * width // CUTS, (i + 1) * width // CUTS) for i in range(CUTS)]
+
+    def y_copy(i, h):
+        return remote(
+            y_out.at[i, :, cuts[h]], y_in.at[i, :, cuts[h]], y_s.at[i, h], y_r.at[i, h], y_peer
+        )
 
     def send_core(i, buf):
         core_out[i, 0] = part[buf, rows_for(t_core), :].astype(bf16)
@@ -693,14 +784,32 @@
 
     def send_y(i, buf):
         core_copy(i).wait_recv()
-        y_out[i] = (part[buf, rows_for(t_y), :] + core_in[i, 1].astype(f32)).astype(bf16)
-        y_copy(i).start()
-        kept[i] = part[buf, rows_for(tp), :] + core_in[i, 0].astype(f32)
-
+        if is_own(i):
+            pair_copy.wait_recv()
+        for h, cols in enumerate(cuts):
+            across = part[buf, rows_for(t_y), cols] + core_in[i, 1, :, cols].astype(f32)
+            along = part[buf, rows_for(tp), cols] + core_in[i, 0, :, cols].astype(f32)
+            if beside(i):
+                pair_out[0, :, cols] = along.astype(bf16)
+                pair_out[1, :, cols] = across.astype(bf16)
+                continue
+            if is_own(i):
+                across = across + pair_in[1, :, cols].astype(f32)
+                along = along + pair_in[0, :, cols].astype(f32)
+            y_out[i, :, cols] = across.astype(bf16)
+            y_copy(i, h).start()
+            kept[i, :, cols] = along
+        if beside(i):
+            pair_copy.start()
+
+    def beside(g):
+        return isinstance(g, int) and g == 1
+
+    pair_copy = remote(pair_out, pair_in, pair_sem.at[2], pair_sem.at[3], at(zx(1), x, tp))
     send_core(zn, 0)
     send_y(zn, 0)
-    forward(arrive[0], wide_two)
-    y_copy(zn).wait_recv()
+    for h in range(CUTS):
+        y_copy(zn, h).wait_recv()
     middle[...] = resid[...].astype(f32) + (kept[zn] + y_in[zn].astype(f32))
     mid_rows = middle[...]
     scale = lax.rsqrt(jnp.mean(mid_rows * mid_rows, axis=-1, keepdims=True) + norm_eps)
@@ -735,6 +844,9 @@
 
     def both_token_came(g):
         return remote(piece(zx(g), t_both), piece(zx(g), t_both), td_s.at[g], td_r.at[g], core_peer)
+
+    def pair_token(zz):
+        return remote(piece(zz, t_y), piece(zz, t_y), pair_sem.at[0], pair_sem.at[1], at(zx(1), x, tp))
 
     def spread_z(g):
         zz = zx(g)
@@ -745,34 +857,45 @@
             up_copy(zz, ring_s.at[g]).wait_recv()
             when((zz < z) & (z < zn - 1), lambda: up_copy(zz, ring_s.at[g]).start())
             when((zz > z) & (z > 0), lambda: down_copy(zz, ring_s.at[g]).start())
-        y_token(g).start()
+        if not beside(g):
+            y_token(g).start()
         core_token(g).start()
 
     def spread_y(g):
-        y_token_came(g).wait_recv()
+        if beside(g):
+            pair_token(zx(1)).wait_recv()
+        else:
+            y_token_came(g).wait_recv()
         both_token(g).start()
+        if is_own(g):
+            pair_token(z).start()
 
     spread_z(own_group)
-    pl.when(z == 0)(lambda: start(z_weights(1)[tall_one]))
-    forward(arrive[0], tall_one)
+    pl.when(z == 0)(lambda: begin(z_weights(1), tall_one, zx(1)))
     if zn > 2:
         forward(arrive[1], every)
     spread_y(0)
     for g in arrive[2:]:
         forward(g, every)
-    for i, g in enumerate(pieces):
-        spread_z(g)
-        if i > 0:
-            spread_y(pieces[i - 1])
-    spread_y(pieces[-1])
-    for c in own_copies[1:]:
-        c.wait()
+    near, far = pieces[0], pieces[1:]
+    spread_z(near)
+    if far:
+        spread_z(far[0])
+
+    @pl.when(inner == 1)
+    def _():
+        for g in far[1:]:
+            spread_z(g)
+        for g in pieces:
+            spread_y(g)
+
+    @pl.when(inner == 0)
+    def _():
+        spread_y(near)
+
+    each(own_copies, every, z, lambda c: c.wait())
     for g in range(zn):
-        for c in x_weights(g):
-            c.wait_recv()
-
-    unit_at = lax.broadcasted_iota(jnp.int32, (1, taken * LANES), 1)
-    mine = unit_at >= jnp.where(z == 0, 0, (first_tile(z - 1) + taken - first_tile(z)) * LANES)
+        each(x_weights(g), every, z, lambda c: c.wait_recv())
 
     def feed(g, buf):
         core_token_came(g).wait_recv()
@@ -780,7 +903,7 @@
         block = tokens[zx(g)]
         gate = mm(block, gbuf[...])
         up = mm(block, ubuf[...])
-        hidden[...] = jnp.where(mine, gate / (1.0 + jnp.exp(-gate)) * up, 0.0).astype(bf16)
+        hidden[...] = (gate / (1.0 + jnp.exp(-gate)) * up).astype(bf16)
 
         def down(i, _):
             cols = pl.ds(pl.multiple_of(i * step, step), step)
@@ -789,51 +912,102 @@
 
         lax.fori_loop(0, width // step, down, 0)
 
-    def z_copy(g):
-        return remote(z_out.at[g], z_in.at[g], z_s.at[g], z_r.at[g], at(zx(g), x, tp))
-
-    def send_z(g):
-        y_copy(g).wait_recv()
-        if is_own(g):
-            kept[g] = kept[g] + y_in[g].astype(f32)
-        else:
-            z_out[g] = (kept[g] + y_in[g].astype(f32)).astype(bf16)
-            z_copy(g).start()
-
-    order = pieces[1:] + pieces[:1] + [own_group]
-    for i, g in enumerate(order):
-        feed(g, i % 2)
-        send_core(g, i % 2)
-        if i >= 1:
-            send_y(order[i - 1], (i - 1) % 2)
-        if i >= 2:
-            send_z(order[i - 2])
-    send_y(order[-1], (zn - 1) % 2)
-    send_z(order[-2])
-    send_z(order[-1])
-    total = middle[...] + kept[0]
+    def z_copy(g, h):
+        return remote(
+            z_out.at[g, :, cuts[h]], z_in.at[g, :, cuts[h]], z_s.at[g, h], z_r.at[g, h],
+            at(zx(g), x, tp),
+        )
+
+    def step_copy(k, g, h):
+        return remote(
+            z_out.at[g, :, cuts[h]], step_in.at[k, :, cuts[h]], z_s.at[g, h], step_r.at[k, h],
+            at(zx(1), x, tp),
+        )
+
+    def send_z(k, g):
+        for h, cols in enumerate(cuts):
+            y_copy(g, h).wait_recv()
+            mine = kept[g, :, cols] + y_in[g, :, cols].astype(f32)
+            if is_own(g):
+                kept[g, :, cols] = mine
+                continue
+
+            @pl.when(inner == 0)
+            def _():
+                z_out[g, :, cols] = mine.astype(bf16)
+                step_copy(k, g, h).start()
+
+            @pl.when(inner == 1)
+            def _():
+                step_copy(k, g, h).wait_recv()
+                z_out[g, :, cols] = (mine + step_in[k, :, cols].astype(f32)).astype(bf16)
+                z_copy(g, h).start()
+
+    feed(near, 2)
+    send_core(near, 2)
+
+    @pl.when(inner == 0)
+    def _():
+        for g in far[1:]:
+            spread_z(g)
+        send_y(near, 2)
+        for g in far[:1]:
+            spread_y(g)
+
+    buf = 0
+    for i, g in enumerate(far):
+        buf = 1 - buf
+        feed(g, buf)
+        send_core(g, buf)
+        if i == 0:
+            pl.when(inner == 1)(lambda: send_y(near, 2))
+        if i + 1 < len(far):
+            send_y(g, buf)
+
+            @pl.when(inner == 0)
+            def _():
+                spread_y(far[i + 1])
+
+    if not far:
+        pl.when(inner == 1)(lambda: send_y(near, 2))
+    feed(own_group, 2)
+    for g in far[-1:]:
+        send_y(g, buf)
+    send_core(own_group, 2)
+    pl.when(inner == 1)(lambda: send_y(own_group, 2))
+    for k, g in enumerate(far):
+        if k + 1 == len(far):
+            pl.when(inner == 0)(lambda: send_y(own_group, 2))
+        send_z(k, g)
+    send_z(0, own_group)
+    for h, cols in enumerate(cuts):
+        z_copy(far[0], h).wait_recv()
+        total = middle[:, cols] + kept[0, :, cols] + z_in[far[0], :, cols].astype(f32)
+        out[:, cols] = total.astype(bf16)
+
     for g in range(1, zn):
-        z_copy(g).wait_recv()
-        total = total + z_in[g].astype(f32)
-    out[...] = total.astype(bf16)
-
-    for g in range(1, zn):
-        for c in z_weights(g):
-            c.wait_send()
-        z_copy(g).wait_send()
+        each(z_weights(g), every, zx(g), lambda c: c.wait_send())
+        for h in range(CUTS):
+            if not beside(g):
+                z_copy(g, h).wait_send()
         zz = zx(g)
         moved_on = ((zz < z) & (z < zn - 1)) | ((zz > z) & (z > 0))
         when(moved_on, up_copy(zz, ring_s.at[g]).wait_send)
     for g in range(zn):
-        for c in x_weights(g):
-            c.wait_send()
-        y_token(g).wait_send()
+        each(x_weights(g), every, z, lambda c: c.wait_send())
+        if not beside(g):
+            y_token(g).wait_send()
         core_token(g).wait_send()
         both_token(g).wait_send()
     for i in range(zn + 1):
         core_copy(i).wait_send()
-        y_copy(i).wait_send()
-    sum_copy.wait_send()
+        for h in range(CUTS):
+            if not beside(i):
+                y_copy(i, h).wait_send()
+    for i in range(pairs // together):
+        sum_copy(i).wait_send()
+    pair_token(z).wait_send()
+    pair_copy.wait_send()
     when(z < zn - 1, state_copy.wait_send)
     when(z < zn - 1, up_copy(z, own_s.at[0]).wait_send)
     when(z > 0, down_copy(z, own_s.at[1]).wait_send)
@@ -847,8 +1021,7 @@
     return (
         tp == 4
         and sp % PAIR == 0
-        and zn > 1
-        and zn & (zn - 1) == 0
+        and zn == 4
         and heads % 2 == 0
         and positions % LANES == 0
         and positions == tp * arrays[0].shape[0]
@@ -893,7 +1066,7 @@
         vmem((pairs, *half), bf16),
         vmem((pairs, *half), f32),
         vmem((positions, channels), bf16),
-        vmem((2, positions, width), f32),
+        vmem((3, positions, width), f32),
         vmem((zn + 1, rows, width), f32),
         vmem((zn + 1, 2, rows, width), bf16),
         vmem((zn + 1, 2, rows, width), bf16),
@@ -904,10 +1077,13 @@
         vmem((rows, width), f32),
         vmem((zn, positions, width), bf16),
         vmem((positions, taken), bf16),
-        dma((4,)),
-        dma((zn, 3)), dma((zn, 3)), dma((zn, 3)), dma((zn, 3)),
-        dma((2,)), dma((2,)),
-        dma((zn + 1,)), dma((zn + 1,)), dma((zn + 1,)), dma((zn + 1,)), dma((zn,)), dma((zn,)),
+        vmem((2, rows, width), bf16),
+        vmem((2, rows, width), bf16),
+        vmem((2, rows, width), bf16),
+        dma((7,)), dma((4,)), dma((2, CUTS)),
+        dma((zn, 6)), dma((zn, 6)), dma((zn, 6)), dma((zn, 6)),
+        dma((2, pairs)), dma((2,)),
+        dma((zn + 1,)), dma((zn + 1,)), dma((zn + 1, CUTS)), dma((zn + 1, CUTS)), dma((zn, CUTS)), dma((zn, CUTS)),
         dma((2,)), dma((zn,)), dma((zn,)),
         dma((zn,)), dma((zn,)), dma((zn,)), dma((zn,)), dma((zn,)), dma((zn,)),
     ]

time: 124 us -> 112 us (0.903)
  Pallas kernels: 122 us -> 110 us
    pallas_call x1, Pallas kernels: 122 us -> 110 us  [fused(): pl.pallas_call(functools.partial(layer_kernel, zn), out_shape=jax.ShapeDt...]
where the time goes in v2:
time: 112 us
  Pallas kernels  110 us (98%)
  local copies, waits for them, and re-layouts  1.67 us (1%)
    pallas_call x1, Pallas kernels, fused(): pl.pallas_call(functools.partial(layer_kernel, zn), out_shape=jax.ShapeDt...  110 us

profile of v2, /device:TPU:0, one launch (start us, length us, event | category | flops | bytes accessed | tf_op | source)
XLA Modules:
  0.0 111.8 jit_solution(15007248181506150028)
XLA Ops:
  0.0 110.1 %layer.1 = bf16[64,2048]{1,0:T(8,128)(2,1)} custom-call(bf16[64,2048]{1,0:T(8,128)(2,1)} %resid.1, bf16[512,256]{1,0:T(8,128)(2,1)} %query.1, bf16[512,256]{1,0:T(8,128)(2,1)} %key.1, bf16[512,256]{1,0:T(8,128)(2,1)} %value.1, bf16[512,256]{1,0:T(8,128)(2,1)} %fading.1, bf16[512,256]{1,0:T(8,128)(2,1)} %step_size.1, bf16[512,256]{1,0:T(8,128)(2,1)} %switch.1, ...), custom_call_target="tpu_custom_call" | custom-call | tf_op jit(solution)/shard_map/layer/pallas_call | solution.py:1092
  110.1 1.7 %copy.17 = bf16[64,2048]{1,0:T(8,128)(2,1)} copy(bf16[64,2048]{1,0:T(8,128)(2,1)} %layer.1) | data formatting | bytes 524288

commit v3 on v2

--- a/solution.py
+++ b/solution.py
@@ -767,8 +767,10 @@
     def rows_for(t):
         return pl.ds(pl.multiple_of(t * rows, rows), rows)
 
-    def core_copy(i):
-        return remote(core_out.at[i], core_in.at[i], core_s.at[i], core_r.at[i], core_peer)
+    def core_copy(i, j):
+        return remote(
+            core_out.at[i, j], core_in.at[i, j], core_s.at[i, j], core_r.at[i, j], core_peer
+        )
 
     cuts = [slice(i * width // CUTS, (i + 1) * width // CUTS) for i in range(CUTS)]
 
@@ -778,26 +780,32 @@
         )
 
     def send_core(i, buf):
+        core_out[i, 1] = part[buf, rows_for(t_both), :].astype(bf16)
+        core_copy(i, 1).start()
         core_out[i, 0] = part[buf, rows_for(t_core), :].astype(bf16)
-        core_out[i, 1] = part[buf, rows_for(t_both), :].astype(bf16)
-        core_copy(i).start()
+        core_copy(i, 0).start()
 
     def send_y(i, buf):
-        core_copy(i).wait_recv()
         if is_own(i):
             pair_copy.wait_recv()
+        core_copy(i, 1).wait_recv()
         for h, cols in enumerate(cuts):
             across = part[buf, rows_for(t_y), cols] + core_in[i, 1, :, cols].astype(f32)
-            along = part[buf, rows_for(tp), cols] + core_in[i, 0, :, cols].astype(f32)
             if beside(i):
-                pair_out[0, :, cols] = along.astype(bf16)
                 pair_out[1, :, cols] = across.astype(bf16)
                 continue
             if is_own(i):
                 across = across + pair_in[1, :, cols].astype(f32)
-                along = along + pair_in[0, :, cols].astype(f32)
             y_out[i, :, cols] = across.astype(bf16)
             y_copy(i, h).start()
+        core_copy(i, 0).wait_recv()
+        for cols in cuts:
+            along = part[buf, rows_for(tp), cols] + core_in[i, 0, :, cols].astype(f32)
+            if beside(i):
+                pair_out[0, :, cols] = along.astype(bf16)
+                continue
+            if is_own(i):
+                along = along + pair_in[0, :, cols].astype(f32)
             kept[i, :, cols] = along
         if beside(i):
             pair_copy.start()
@@ -1000,7 +1008,8 @@
         core_token(g).wait_send()
         both_token(g).wait_send()
     for i in range(zn + 1):
-        core_copy(i).wait_send()
+        for j in range(2):
+            core_copy(i, j).wait_send()
         for h in range(CUTS):
             if not beside(i):
                 y_copy(i, h).wait_send()
@@ -1083,7 +1092,7 @@
         dma((7,)), dma((4,)), dma((2, CUTS)),
         dma((zn, 6)), dma((zn, 6)), dma((zn, 6)), dma((zn, 6)),
         dma((2, pairs)), dma((2,)),
-        dma((zn + 1,)), dma((zn + 1,)), dma((zn + 1, CUTS)), dma((zn + 1, CUTS)), dma((zn, CUTS)), dma((zn, CUTS)),
+        dma((zn + 1, 2)), dma((zn + 1, 2)), dma((zn + 1, CUTS)), dma((zn + 1, CUTS)), dma((zn, CUTS)), dma((zn, CUTS)),
         dma((2,)), dma((zn,)), dma((zn,)),
         dma((zn,)), dma((zn,)), dma((zn,)), dma((zn,)), dma((zn,)), dma((zn,)),
     ]

time: 112 us -> 112 us (level)
  no operation moved by 1% of the time
where the time goes in v3:
time: 112 us
  Pallas kernels  111 us (99%)
  local copies, waits for them, and re-layouts  1.67 us (1%)
    pallas_call x1, Pallas kernels, fused(): pl.pallas_call(functools.partial(layer_kernel, zn), out_shape=jax.ShapeDt...  111 us

profile of v3, /device:TPU:0, one launch (start us, length us, event | category | flops | bytes accessed | tf_op | source)
XLA Modules:
  0.0 112.2 jit_solution(14930761892296508436)
XLA Ops:
  0.0 110.6 %layer.1 = bf16[64,2048]{1,0:T(8,128)(2,1)} custom-call(bf16[64,2048]{1,0:T(8,128)(2,1)} %resid.1, bf16[512,256]{1,0:T(8,128)(2,1)} %query.1, bf16[512,256]{1,0:T(8,128)(2,1)} %key.1, bf16[512,256]{1,0:T(8,128)(2,1)} %value.1, bf16[512,256]{1,0:T(8,128)(2,1)} %fading.1, bf16[512,256]{1,0:T(8,128)(2,1)} %step_size.1, bf16[512,256]{1,0:T(8,128)(2,1)} %switch.1, ...), custom_call_target="tpu_custom_call" | custom-call | tf_op jit(solution)/shard_map/layer/pallas_call | solution.py:1101
  110.6 1.7 %copy.17 = bf16[64,2048]{1,0:T(8,128)(2,1)} copy(bf16[64,2048]{1,0:T(8,128)(2,1)} %layer.1) | data formatting | bytes 524288
